TPU v7x, 256 devices: a whole 4x4x8 slice. The times are simulated.
256 devices in a mesh: dp: 4 (over x), kv: 32 (over z, y), tp: 2 (over core).
Axes of the slice: x: 4, y: 4, z: 8, core: 2. Of those that a mesh axis runs over, the one named last changes fastest.
Arguments:
- tokens: bfloat16 [4, 8192, 1024], P('dp', 'kv', 'tp'), may hold values from -6 to 6
- norm_gain: float32 [1024], replicated, may hold values from 0.1 to 1.9
- w_query: bfloat16 [1024, 1024], P(None, 'tp'), may hold values from -0.1875 to 0.1875
- w_key: bfloat16 [1024, 256], P(None, 'tp'), may hold values from -0.1875 to 0.1875
- w_value: bfloat16 [1024, 256], P(None, 'tp'), may hold values from -0.1875 to 0.1875
- q_gain: float32 [64], replicated, may hold values from 0.1 to 1.9
- k_gain: float32 [64], replicated, may hold values from 0.1 to 1.9
- w_out: bfloat16 [1024, 1024], P('tp'), may hold values from -4 to 4
- chosen: int32 [4, 256, 16], P('dp', 'kv'), may hold values from -1 to 255, as said below
Outputs:
- mixed: bfloat16 [4, 8192, 1024], P('dp', 'kv', 'tp')
- log_total: float32 [4, 16, 8192], P('dp', 'tp', 'kv')
Inputs may be any that keep to these rules, and one draw needn't show every extreme that they name: Each row of chosen (one query block b) holds distinct key block numbers, all at most b, and -1 for empty entries; b itself is always present; a row is full (16 blocks) whenever at least 16 blocks may be chosen by it. Over the 8 rows of one index of kv, the chosen blocks that lie on any one other index of kv are at most 4 distinct ones, and exactly 4 of those on the index just before, for every index but the first. Some blocks are chosen far more often than others.
All inputs are finite; a program needn't handle non-finite values.
Results may differ from a plain program's by a relative error of at most 0.015.
Values may be sent and summed in bfloat16 or wider, within the bound.
A program may use at most 64 MiB of HBM per device.

v0:
```python
import math

import jax
import jax.numpy as jnp
from jax import lax
from jax.sharding import Mesh
from jax.sharding import PartitionSpec as P

H = 16
HD = 64
BLK = 32
KV = ("kv_0", "kv_1")


epsilon = 1e-06
alibi_reach = 4.0
masked = -1e30


def whole_of(value, axes, dim):
    result = value
    for number in range(len(axes) - 1, -1, -1):
        result = lax.all_gather(result, axes[number], axis=dim, tiled=True)
    return result


def rms_norm(values, gain):
    return (
        values
        * lax.rsqrt(jnp.mean(values * values, axis=-1, keepdims=True) + epsilon)
        * gain.astype(jnp.float32)
    )


def body(tokens, norm_gain, w_query, w_key, w_value, q_gain, k_gain, w_out, chosen):
    gathered = lax.all_gather(tokens, "tp", axis=2, tiled=True)
    seq_dev, tok_dev, model_width = gathered.shape
    n_kv = lax.axis_size(KV)
    n_tp = lax.axis_size("tp")
    kv_index = lax.axis_index(KV)
    tp_index = lax.axis_index("tp")
    heads_here = w_query.shape[1] // HD
    kv_here = w_key.shape[1] // HD
    group_size = heads_here // kv_here
    blocks_here = tok_dev // BLK
    seq_len = tok_dev * n_kv
    hidden = (
        rms_norm(gathered.astype(jnp.float32), norm_gain)
        .astype(jnp.bfloat16)
        .reshape(seq_dev * tok_dev, model_width)
    )
    queries = rms_norm(
        jnp.dot(hidden, w_query, preferred_element_type=jnp.float32).reshape(
            seq_dev, tok_dev, heads_here, HD
        ),
        q_gain,
    ).astype(jnp.bfloat16)
    key_rows = rms_norm(
        jnp.dot(hidden, w_key, preferred_element_type=jnp.float32).reshape(
            seq_dev, tok_dev, kv_here, HD
        ),
        k_gain,
    ).astype(jnp.bfloat16)
    value_rows = (
        jnp.dot(hidden, w_value, preferred_element_type=jnp.float32)
        .astype(jnp.bfloat16)
        .reshape(seq_dev, tok_dev, kv_here, HD)
    )
    queries = queries.reshape(seq_dev, blocks_here, BLK, kv_here, group_size, HD)
    head_ids = tp_index * heads_here + jnp.arange(heads_here, dtype=jnp.int32)
    slopes = jnp.exp2(-8.0 * (head_ids + 1).astype(jnp.float32) / H).reshape(kv_here, group_size)
    query_pos = (kv_index * tok_dev + jnp.arange(tok_dev, dtype=jnp.int32)).reshape(
        blocks_here, BLK
    )
    score_scale = HD ** (-0.5)

    def absorb(state_now, span_keys, span_values, key_pos, usable):
        row_max, row_sum, weighted = state_now
        key_block = key_pos // BLK
        member = jnp.any(chosen[:, :, :, None] == key_block[:, None, None, :], axis=2)
        offset = query_pos[None, :, :, None] - key_pos[:, None, None, :]
        allowed = member[:, :, None, :] & usable[:, None, None, :] & (offset >= 0)
        scores = (
            jnp.einsum(
                "sbqkgd,snkd->skgbqn", queries, span_keys, preferred_element_type=jnp.float32
            )
            * score_scale
        )
        penalty = (
            slopes[None, :, :, None, None, None]
            * offset.astype(jnp.float32)[:, None, None]
            * alibi_reach
            / seq_len
        )
        scores = jnp.where(allowed[:, None, None], scores - penalty, masked)
        new_max = jnp.maximum(row_max, jnp.max(scores, axis=-1))
        weights = jnp.where(allowed[:, None, None], jnp.exp(scores - new_max[..., None]), 0.0)
        shrink = jnp.exp(row_max - new_max)
        row_sum = row_sum * shrink + jnp.sum(weights, axis=-1)
        weighted = weighted * shrink[..., None] + jnp.einsum(
            "skgbqn,snkd->skgbqd",
            weights.astype(jnp.bfloat16),
            span_values,
            preferred_element_type=jnp.float32,
        )
        return (new_max, row_sum, weighted)

    stat_shape = (seq_dev, kv_here, group_size, blocks_here, BLK)
    initial = (
        jnp.full(stat_shape, masked, jnp.float32),
        jnp.zeros(stat_shape, jnp.float32),
        jnp.zeros(stat_shape + (HD,), jnp.float32),
    )

    def fold_piece(state_now, shard_piece, first_row):
        piece_keys, piece_values = shard_piece
        row_count = piece_keys.shape[1]
        span_len = math.gcd(row_count, tok_dev)

        def one_span(step_index, running):
            first_key = step_index * span_len
            span_keys = lax.dynamic_slice_in_dim(piece_keys, first_key, span_len, 1)
            span_values = lax.dynamic_slice_in_dim(piece_values, first_key, span_len, 1)
            key_pos = jnp.broadcast_to(
                first_row.astype(jnp.int32) + first_key + jnp.arange(span_len, dtype=jnp.int32),
                (seq_dev, span_len),
            )
            return absorb(
                running, span_keys, span_values, key_pos, jnp.ones((seq_dev, span_len), bool)
            )

        return lax.fori_loop(0, row_count // span_len, one_span, state_now)

    row_max, row_sum, weighted = fold_piece(
        initial, (whole_of(key_rows, KV, 1), whole_of(value_rows, KV, 1)), jnp.int32(0)
    )
    attended = (weighted / row_sum[..., None]).transpose(0, 3, 4, 1, 2, 5)
    attended = attended.reshape(seq_dev * tok_dev, heads_here * HD).astype(jnp.bfloat16)
    log_total = (row_max + jnp.log(row_sum)).reshape(seq_dev, heads_here, tok_dev)
    own_rows = model_width // n_tp

    def project():
        out_cols = lax.slice_in_dim(w_out, 0, lax.axis_size("tp") * own_rows, axis=1)
        return jnp.dot(attended, out_cols, preferred_element_type=jnp.float32).T

    scattered = lax.psum_scatter(
        project().astype(jnp.bfloat16), "tp", scatter_dimension=0, tiled=True
    ).astype(jnp.float32)
    mixed = scattered.T.reshape(seq_dev, tok_dev, own_rows).astype(jnp.bfloat16)
    return (mixed, log_total)


def solution(mesh):
    split = Mesh(
        mesh.devices.reshape(mesh.shape["dp"], 8, 4, mesh.shape["tp"]), ("dp", "kv_0", "kv_1", "tp")
    )
    placed = (
        P("dp", KV, "tp"),
        P(),
        P(None, "tp"),
        P(None, "tp"),
        P(None, "tp"),
        P(),
        P(),
        P("tp", None),
        P("dp", KV, None),
    )
    return jax.shard_map(
        body,
        mesh=split,
        in_specs=placed,
        out_specs=(P("dp", KV, "tp"), P("dp", "tp", KV)),
        check_vma=False,
    )
```

profile of v0, /device:TPU:1, one launch (start us, length us, event | category | flops | bytes accessed | tf_op | source)
XLA Modules:
  0.0 281.3 jit_solution(15740097225151936718)
XLA Ops:
  7.3 5.3 %all_gather.15 = bf16[1,256,1024]{2,1,0:T(8,128)(2,1)S(1)} all-gather(bf16[1,256,512]{2,1,0:T(8,128)(2,1)} %param.11), channel_id=1, replica_groups=mesh['dp'=4,'kv_0'=8,'kv_1'=4,'tp'=2] {'tp'}, dimensions={2}, use_global_device_ids=true | all-gather | bytes 786432 | tf_op jit(solution)/shard_map/all_gather | solution.py:36
  14.3 10.1 %all_gather.16 = bf16[1,1024,2,64]{1,3,2,0:T(8,128)(2,1)} all-gather(bf16[1,256,2,64]{1,3,2,0:T(8,128)(2,1)S(1)} %multiply_convert_fusion), channel_id=1, replica_groups=mesh['dp'=4,'kv_0'=8,'kv_1'=4,'tp'=2] {'kv_1'}, dimensions={1}, use_global_device_ids=true | all-gather | bytes 327680 | tf_op jit(solution)/shard_map/all_gather | solution.py:23
  24.9 10.1 %all_gather.18 = bf16[1,1024,2,64]{1,3,2,0:T(8,128)(2,1)} all-gather(bf16[1,256,2,64]{1,3,2,0:T(8,128)(2,1)S(1)} %bitcast.99), channel_id=1, replica_groups=mesh['dp'=4,'kv_0'=8,'kv_1'=4,'tp'=2] {'kv_1'}, dimensions={1}, use_global_device_ids=true | all-gather | bytes 327680 | tf_op jit(solution)/shard_map/all_gather | solution.py:23
  36.8 1.6 reshape.336
  39.6 25.4 %all-gather.3.cloned.1.call-done = bf16[1,8192,2,64]{1,3,2,0:T(8,128)(2,1)} async-done(((bf16[1,1024,2,64]{1,3,2,0:T(8,128)(2,1)}), bf16[1,8192,2,64]{1,3,2,0:T(8,128)(2,1)}) %all-gather.3.cloned.1.call-update) | async-done | bytes 2097168 | tf_op jit(solution)/shard_map/all_gather | solution.py:23
  64.9 41.0 %all-gather.5.cloned.1.call-done = bf16[1,8192,2,64]{1,3,2,0:T(8,128)(2,1)} async-done(((bf16[1,1024,2,64]{1,3,2,0:T(8,128)(2,1)}), bf16[1,8192,2,64]{1,3,2,0:T(8,128)(2,1)}) %all-gather.5.cloned.1.call-update) | async-done | bytes 2097168 | tf_op jit(solution)/shard_map/all_gather | solution.py:23
  105.9 149.5 %while.20 = (s32[]{:T(128)}, f32[1,2,4,8,32]{4,2,3,1,0:T(4,128)S(1)}, f32[1,2,4,8,32]{4,2,3,1,0:T(4,128)S(1)}, f32[1,2,4,8,32,64]{5,4,3,2,1,0:T(8,128)S(1)}, s32...) while((s32[]{:T(128)}, ...), condition=%wide.region_7.8_spmd.clone, body=%wide.region_3.7_spmd.clone.sunk | while | flops 140261664 | bytes 8870747 | solution.py:132
  106.5 1.7 fusion.49
  109.1 1.4 fusion.52
  111.1 1.7 fusion.49
  115.8 1.7 fusion.49
  120.5 1.7 fusion.49
  123.2 1.4 fusion.52
  125.2 1.7 fusion.49
  127.8 1.4 fusion.52
  129.8 1.7 fusion.49
  132.5 1.4 fusion.52
  134.5 1.7 fusion.49
  139.2 1.7 fusion.49
  143.9 1.7 fusion.49
  146.5 1.4 fusion.52
  148.5 1.7 fusion.49
  151.2 1.4 fusion.52
  153.2 1.7 fusion.49
  157.9 1.7 fusion.49
  162.5 1.7 fusion.49
  167.2 1.7 fusion.49
  169.9 1.4 fusion.52
  171.9 1.7 fusion.49
  174.6 1.4 fusion.52
  176.6 1.7 fusion.49
  181.2 1.7 fusion.49
  185.9 1.7 fusion.49
  190.6 1.7 fusion.49
  195.3 1.7 fusion.49
  199.9 1.7 fusion.49
  204.6 1.7 fusion.49
  209.3 1.7 fusion.49
  214.0 1.7 fusion.49
  218.6 1.7 fusion.49
  223.3 1.7 fusion.49
  228.0 1.7 fusion.49
  232.7 1.7 fusion.49
  237.3 1.7 fusion.49
  242.0 1.7 fusion.49
  246.7 1.7 fusion.49
  251.3 1.7 fusion.49
  258.6 16.2 %reduce-scatter.2.cloned.1.call-done = bf16[512,256]{0,1:T(8,128)(2,1)} async-done(((bf16[1024,256]{0,1:T(8,128)(2,1)}), bf16[512,256]{0,1:T(8,128)(2,1)}) %reduce-scatter.2.cloned.1.call-update) | async-done | bytes 262160 | tf_op jit(solution)/shard_map/reduce_scatter | solution.py:146
  (485 shorter events, 87.7 us)
Async XLA Ops:
  7.2 28.0 %copy-start = (bf16[1024,512]{1,0:T(8,128)(2,1)S(1)}, bf16[1024,512]{1,0:T(8,128)(2,1)}, u32[]{:S(2)}) copy-start(bf16[1024,512]{1,0:T(8,128)(2,1)} %param.13) | copy-start | bytes 3145732
  7.2 17.3 %copy-start.3 = (f32[1024]{0:T(1024)S(1)}, f32[1024]{0:T(1024)}, u32[]{:S(2)}) copy-start(f32[1024]{0:T(1024)} %param.12) | copy-start | bytes 12292
  7.2 7.0 %copy-start.4 = (f32[64]{0:T(128)S(1)}, f32[64]{0:T(128)}, u32[]{:S(2)}) copy-start(f32[64]{0:T(128)} %param.17) | copy-start | bytes 772
  7.2 17.3 %copy-start.6 = (bf16[1024,128]{1,0:T(8,128)(2,1)S(1)}, bf16[1024,128]{1,0:T(8,128)(2,1)}, u32[]{:S(2)}) copy-start(bf16[1024,128]{1,0:T(8,128)(2,1)} %param.15) | copy-start | bytes 786436
  7.2 57.7 %all-gather.3.cloned.1.call-start = ((), (), s32[]{:S(2)}) async-start(), calls=%async_computation.1 | async-start | bytes 2359296 | tf_op jit(solution)/shard_map/all_gather | solution.py:23
  24.4 81.5 %all-gather.5.cloned.1.call-start = ((), (), s32[]{:S(2)}) async-start(), calls=%async_computation.2 | async-start | bytes 2359296 | tf_op jit(solution)/shard_map/all_gather | solution.py:23
  35.0 239.8 %reduce-scatter.2.cloned.1.call-start = ((), (), s32[]{:S(2)}) async-start(), calls=%async_computation.3 | async-start | bytes 786432 | tf_op jit(solution)/shard_map/reduce_scatter | solution.py:146
  36.4 2.0 copy-start.5
  36.6 69.3 %copy-start.2 = (s32[1,8,16]{2,1,0:T(8,128)S(1)}, s32[1,8,16]{2,1,0:T(8,128)}, u32[]{:S(2)}) copy-start(s32[1,8,16]{2,1,0:T(8,128)} %param.19) | copy-start | bytes 1540
  255.5 1.2 copy-start.1
Sparse Core Ops, SparseCore 0:
  24.5 40.3 all-gather.2
  66.7 39.1 all-gather.4
  258.1 16.7 reduce-scatter.1
where the time goes:
time: 284 us; the launch traced here: 281 us
  matrix products  105 us (37%)
  waiting for transfers between devices  82.6 us (29%)
  other arithmetic  42.3 us (15%)
  blocking collectives  25.5 us (9%)
  between operations  14 us (5%)
  local copies, waits for them, and re-layouts  8.75 us (3%)
  loops' own time  2.92 us (1%)
    all_gather x2, waiting for transfers between devices, whole_of(): result = lax.all_gather(result, axes[number], axis=dim, tiled=True)  66.4 us
    dot_general x32, matrix products, absorb(): jnp.einsum('sbqkgd,snkd->skgbqn', queries, span_keys, preferred_element_t...  55.8 us
    dot_general x32, matrix products, absorb(): jnp.einsum('skgbqn,snkd->skgbqd', weights.astype(jnp.bfloat16), span_valu...  45 us
    another operation x32, other arithmetic  26.6 us
    all_gather x2, blocking collectives, whole_of(): result = lax.all_gather(result, axes[number], axis=dim, tiled=True)  20.2 us
    reduce_scatter x1, waiting for transfers between devices, body(): lax.psum_scatter(project().astype(jnp.bfloat16), 'tp', scatter_dimension=...  16.2 us
  transfers between devices with their start and end apart: 3, of which 3 were waited for; matrix products, arithmetic and copies ran while one was open for 2% of the time, Pallas kernels for 0%

commit v1 on v0

v1 whole, which is shorter than its diff:
```python
import functools
import math

import jax
import jax.numpy as jnp
from jax import lax
from jax.experimental import pallas as pl
from jax.experimental.pallas import tpu as pltpu
from jax.sharding import PartitionSpec as P

MESH = pl.DeviceIdType.MESH
F32 = jnp.float32
BF16 = jnp.bfloat16
I32 = jnp.int32

NZ, NY = 8, 4
NB = 8
BLK = 32
TOPB = 16
MOST = 4
HD = 64
HEADS = 8
TOK = NB * BLK
EPS = 1e-6
SEQ = 8192
OWN = NZ * NY * MOST
LANDED = OWN + NB
FAR = -1e30
PAIRS = ((0, 5), (2, 7), (1, 4), (3, 6))
LOG2E = math.log2(math.e)


def half_sums(x):
    row = lax.broadcasted_iota(I32, (128, 128), 0) // HD
    col = lax.broadcasted_iota(I32, (128, 128), 1) // HD
    ones = jnp.where(row == col, 1.0, 0.0).astype(BF16)
    high = x.astype(BF16)
    low = (x - high.astype(F32)).astype(BF16)
    return jnp.dot(high, ones, preferred_element_type=F32) + jnp.dot(
        low, ones, preferred_element_type=F32
    )


def head_norm(x, gain):
    return x * lax.rsqrt(half_sums(x * x) * (1.0 / HD) + EPS) * gain


def kernel(
    tokens, gain, wq, wk, wv, qg, kg, wo, chosen,
    out, logs,
    tok, hid, wq_v, wkv_v, wo_v,
    c0, c1, c2, c3, c4, c5, c6, c7,
    msg, land, sel_v, nsel_v, ent_v, sel_s, nsel_s, ent_s,
    upos, bias_t, bias_a, qbd, kvg, att, lsum, part, part_in,
    load_sem, tab_sem, tok_send, tok_recv, nsel_send, nsel_recv,
    up_send, up_recv, dn_send, dn_recv, y_send, y_recv, out_send, out_recv,
):
    dp = lax.axis_index("dp")
    kv = lax.axis_index("kv")
    tp = lax.axis_index("tp")
    z = kv // NY
    y = kv % NY
    col = (c0, c1, c2, c3, c4, c5, c6, c7)

    def dev(dz, dy):
        return (dp, ((z + dz) % NZ) * NY + (y + dy) % NY, tp)

    partner = (dp, kv, 1 - tp)

    def remote(src, dst, send, recv, where):
        return pltpu.make_async_remote_copy(
            src_ref=src, dst_ref=dst, send_sem=send, recv_sem=recv,
            device_id=where, device_id_type=MESH,
        )

    loads = [
        pltpu.make_async_copy(tokens, tok.at[tp], load_sem.at[0]),
        pltpu.make_async_copy(wk, wkv_v.at[:, pl.ds(0, 128)], load_sem.at[1]),
        pltpu.make_async_copy(wv, wkv_v.at[:, pl.ds(128, 128)], load_sem.at[2]),
        pltpu.make_async_copy(wq, wq_v, load_sem.at[3]),
    ]
    for p, pair in enumerate(PAIRS):
        for side in range(2):
            loads.append(
                pltpu.make_async_copy(
                    wo.at[pl.ds(pair[side] * HD, HD), :],
                    wo_v.at[pl.ds(p * 128 + side * HD, HD), :],
                    load_sem.at[4 + 2 * p + side],
                )
            )
    for load in loads:
        load.start()

    barrier = pltpu.get_barrier_semaphore()
    peers = [partner, dev(0, 1), dev(0, 2), dev(0, 3), dev(1, 0), dev(-1, 0)]
    for peer in peers:
        pl.semaphore_signal(barrier, inc=1, device_id=peer, device_id_type=MESH)
    pl.semaphore_wait(barrier, len(peers))

    tok_copy = remote(tokens, tok.at[tp], tok_send.at[0], tok_recv.at[0], partner)
    tok_copy.start()

    ch = chosen[...]
    lane = lax.broadcasted_iota(I32, (NB, 256), 1)
    own_block = kv * NB + lax.broadcasted_iota(I32, (NB, 1), 0)
    member = jnp.zeros((NB, 256), I32)
    for e in range(TOPB):
        member = jnp.where(ch[:, e : e + 1] == lane, 1, member)
    present = jnp.broadcast_to(jnp.max(member, axis=0, keepdims=True), (NB, 256))
    inner = lane % NB
    rank = jnp.zeros((NB, 256), I32)
    for k in range(1, NB):
        rank = rank + jnp.where(inner >= k, pltpu.roll(present, k, 1), 0)
    sub = lax.broadcasted_iota(I32, (NB, 256), 0)
    sel = jnp.zeros((NB, 256), I32)
    for s in range(MOST):
        val = jnp.where((present == 1) & (rank == s), inner, 0)
        for k in (1, 2, 4):
            val = val + pltpu.roll(val, 256 - k, 1)
        sel = jnp.where(sub == s, val, sel)
    sel_v[...] = sel
    chip = lane // NB
    from_y = (y - chip % NY + NY) % NY
    from_z = (z - chip // NY + NZ) % NZ
    spot_of = jnp.where(
        chip == kv,
        OWN + inner,
        (from_y * NZ + from_z) * MOST + rank,
    )
    front = jnp.where(
        lax.broadcasted_iota(I32, (NB, TOPB), 1) == 0,
        own_block,
        jnp.where(ch == own_block, ch[:, 0:1], ch),
    )
    filled = jnp.where(front < 0, own_block, front)
    lane_e = lax.broadcasted_iota(I32, (NB, 128), 1)
    entry = jnp.zeros((NB, 128), I32)
    lane_u = lax.broadcasted_iota(I32, (NB, TOPB * BLK), 1)
    pos = jnp.full((NB, TOPB * BLK), FAR, F32)
    for e in range(TOPB):
        at = jnp.sum(jnp.where(filled[:, e : e + 1] == lane, spot_of, 0), axis=1, keepdims=True)
        entry = jnp.where(lane_e == e, at, entry)
        first = front[:, e : e + 1]
        pos = jnp.where(
            (lane_u // BLK == e) & (first >= 0),
            (first * BLK + lane_u % BLK).astype(F32),
            pos,
        )
    ent_v[...] = entry
    for r in range(NB):
        upos[r] = jnp.broadcast_to(pos[r : r + 1], (8, TOPB * BLK))

    nsel_copies = []
    for dy in range(1, NY):
        c = remote(sel_v, nsel_v.at[dy], nsel_send.at[dy], nsel_recv.at[dy], dev(0, dy))
        c.start()
        nsel_copies.append(c)
    tabs = [
        pltpu.make_async_copy(sel_v, sel_s, tab_sem.at[0]),
        pltpu.make_async_copy(ent_v, ent_s, tab_sem.at[1]),
    ]
    for t in tabs:
        t.start()

    rows = lax.broadcasted_iota(I32, (TOK, 128), 0)
    head_no = (tp * HEADS + rows // BLK + 1).astype(F32)
    bias_t[...] = (rows % BLK).astype(F32)
    bias_a[...] = jnp.exp2(head_no * (-8.0 / 16.0)) * (4.0 / SEQ * LOG2E)
    lsum[...] = jnp.zeros((TOK, 256), F32)

    loads[0].wait()
    tok_copy.wait_recv()
    g0 = gain[:, 0:512]
    g1 = gain[:, 512:1024]

    def norm_rows(i, carry):
        at = pl.ds(i * 32, 32)
        a = tok[0, at, :].astype(F32)
        b = tok[1, at, :].astype(F32)
        total = jnp.sum(a * a + b * b, axis=1, keepdims=True)
        r = lax.rsqrt(total * (1.0 / 1024.0) + EPS)
        hid[at, 0:512] = (a * r * g0).astype(BF16)
        hid[at, 512:1024] = (b * r * g1).astype(BF16)
        return carry

    lax.fori_loop(0, 8, norm_rows, 0)
    loads[1].wait()
    loads[2].wait()
    kgain = jnp.concatenate([kg[...], kg[...]], axis=1)
    qgain = jnp.concatenate([qg[...], qg[...]], axis=1)
    both = jnp.dot(hid[...], wkv_v[...], preferred_element_type=F32)
    keys = head_norm(both[:, 0:128], kgain).astype(BF16)
    values = both[:, 128:256].astype(BF16)
    for k, rows_of in enumerate((keys, values)):
        blocks = rows_of.reshape(NB, BLK, 128)
        c0[:, :, 128 * k : 128 * (k + 1)] = blocks
        land[pl.ds(OWN, NB), :, 128 * k : 128 * (k + 1)] = blocks

    def up(d, half):
        at = pl.ds(half * 4, 4)
        return remote(
            col[d].at[at], col[d + 1].at[at],
            up_send.at[2 * d + half], up_recv.at[2 * d + half], dev(1, 0),
        )

    def down(d, half):
        at = pl.ds(half * 4, 4)
        return remote(
            col[(8 - d) % 8].at[at], col[7 - d].at[at],
            dn_send.at[2 * d + half], dn_recv.at[2 * d + half], dev(-1, 0),
        )

    ups = [[up(d, half) for half in range(2)] for d in range(4)]
    downs = [[down(d, half) for half in range(2)] for d in range(3)]
    for half in range(2):
        ups[0][half].start()
        downs[0][half].start()

    y_copies = {}

    def pick(d, dy):
        source = (((z - d + NZ) % NZ) * NY + y) * NB
        for s in range(MOST):
            which = sel_s[s, source] if dy == 0 else nsel_s[dy, s, source]
            block = col[d][which]
            if dy == 0:
                land[d * MOST + s] = block
            else:
                msg[dy * NZ + d, s] = block

    def serve(d):
        for dy in range(1, NY):
            pick(d, dy)
        for dy in range(1, NY):
            k = dy * NZ + d
            c = remote(
                msg.at[k], land.at[pl.ds(k * MOST, MOST)],
                y_send.at[k], y_recv.at[k], dev(0, dy),
            )
            c.start()
            y_copies[k] = c
        if d:
            pick(d, 0)

    for c in nsel_copies:
        c.wait_recv()
    ntab = [
        pltpu.make_async_copy(nsel_v.at[NY - dy], nsel_s.at[dy], tab_sem.at[1 + dy])
        for dy in range(1, NY)
    ]
    for t in ntab:
        t.start()
    for t in tabs + ntab:
        t.wait()
    serve(0)

    loads[3].wait()
    flat = jnp.dot(hid[...], wq_v[...], preferred_element_type=F32)
    normed = [head_norm(flat[:, 128 * t : 128 * (t + 1)], qgain) for t in range(4)]
    low_half = lax.broadcasted_iota(I32, (TOK, 128), 1) < HD
    turned = [pltpu.roll(x, HD, 1) for x in normed]
    paired = (
        jnp.where(low_half, normed[0], normed[2]),
        jnp.where(low_half, normed[1], normed[3]),
        jnp.where(low_half, turned[0], turned[2]),
        jnp.where(low_half, turned[1], turned[3]),
    )
    for p, pair in enumerate(PAIRS):
        first = jnp.where(low_half, paired[p], 0.0).astype(BF16)
        second = jnp.where(low_half, 0.0, paired[p]).astype(BF16)
        for r in range(NB):
            qbd[r, pl.ds(pair[0] * BLK, BLK), :] = first[r * BLK : (r + 1) * BLK]
            qbd[r, pl.ds(pair[1] * BLK, BLK), :] = second[r * BLK : (r + 1) * BLK]

    for k in range(1, 5):
        for half in range(2):
            ups[k - 1][half].wait_recv()
            if k < 4:
                ups[k][half].start()
            if k < 4:
                downs[k - 1][half].wait_recv()
                if k < 3:
                    downs[k][half].start()
        serve(k)
        if k < 4:
            serve(8 - k)
    for load in loads[4:]:
        load.wait()
    for c in y_copies.values():
        c.wait_recv()

    def attend(r, carry):
        for e in range(TOPB):
            kvg[pl.ds(e * BLK, BLK), :] = land[ent_s[r, e]]
        raw = lax.dot_general(
            qbd[r], kvg[:, 0:128], (((1,), (1,)), ((), ())), preferred_element_type=F32
        )
        t = bias_t[...] + ((kv * NB + r) * BLK).astype(F32)
        a = bias_a[...]
        total = jnp.zeros((TOK, 128), F32)
        probs = []
        for i in range(4):
            u = upos[r, 0:1, 128 * i : 128 * (i + 1)]
            if i == 0:
                off = jnp.where(u > t, FAR, u - t)
            else:
                off = u - t
            w = jnp.exp2(raw[:, 128 * i : 128 * (i + 1)] * (LOG2E / 8.0) + a * off)
            total = total + w
            probs.append(w.astype(BF16))
        row_sum = jnp.sum(total, axis=1, keepdims=True)
        weighted = jnp.dot(
            jnp.concatenate(probs, axis=1), kvg[:, 128:256], preferred_element_type=F32
        )
        weighted = weighted / row_sum
        low = lax.broadcasted_iota(I32, (BLK, 128), 1) < HD
        for p, pair in enumerate(PAIRS):
            tile = jnp.where(
                low,
                weighted[pair[0] * BLK : (pair[0] + 1) * BLK],
                weighted[pair[1] * BLK : (pair[1] + 1) * BLK],
            )
            att[pl.ds(pl.multiple_of(r * BLK, BLK), BLK), 128 * p : 128 * (p + 1)] = tile.astype(
                BF16
            )
        spot = lax.broadcasted_iota(I32, (TOK, 256), 1)
        query = lax.broadcasted_iota(I32, (TOK, 256), 0) % BLK
        lsum[...] = jnp.where(spot == r * BLK + query, row_sum, lsum[...])
        return carry

    out_copies = []
    for piece in range(2):
        lax.fori_loop(piece * 4, piece * 4 + 4, attend, 0)
        at = pl.ds(piece * 128, 128)
        rows_in = att[at, :]
        theirs = pl.multiple_of((1 - tp) * 512, 512)
        part[at, :] = jnp.dot(
            rows_in, wo_v[:, pl.ds(theirs, 512)], preferred_element_type=F32
        ).astype(BF16)
        c = remote(
            part.at[at, :], part_in.at[at, :], out_send.at[piece], out_recv.at[piece], partner
        )
        c.start()
        out_copies.append(c)
    logs[...] = jnp.log(jnp.sum(lsum[...].reshape(HEADS, BLK, 256), axis=1))
    mine = pl.multiple_of(tp * 512, 512)
    for piece in range(2):
        at = pl.ds(piece * 128, 128)
        own = jnp.dot(att[at, :], wo_v[:, pl.ds(mine, 512)], preferred_element_type=F32)
        out_copies[piece].wait_recv()
        out[at, :] = (own + part_in[at, :].astype(F32)).astype(BF16)

    tok_copy.wait_send()
    for c in nsel_copies + out_copies + list(y_copies.values()):
        c.wait_send()
    for pair in ups + downs:
        for c in pair:
            c.wait_send()


def body(tokens, norm_gain, w_query, w_key, w_value, q_gain, k_gain, w_out, chosen):
    any_space = pl.BlockSpec(memory_space=pl.ANY)
    vmem = pl.BlockSpec(memory_space=pltpu.VMEM)
    dma = pltpu.SemaphoreType.DMA
    mixed, logs = pl.pallas_call(
        kernel,
        out_shape=(
            jax.ShapeDtypeStruct((TOK, 512), BF16),
            jax.ShapeDtypeStruct((HEADS, TOK), F32),
        ),
        in_specs=[any_space, vmem, any_space, any_space, any_space, vmem, vmem, any_space, vmem],
        out_specs=(vmem, vmem),
        scratch_shapes=[
            pltpu.VMEM((2, TOK, 512), BF16),
            pltpu.VMEM((TOK, 1024), BF16),
            pltpu.VMEM((1024, 512), BF16),
            pltpu.VMEM((1024, 256), BF16),
            pltpu.VMEM((512, 1024), BF16),
            *[pltpu.VMEM((NB, BLK, 256), BF16) for _ in range(8)],
            pltpu.VMEM((NZ * NY, MOST, BLK, 256), BF16),
            pltpu.VMEM((LANDED, BLK, 256), BF16),
            pltpu.VMEM((NB, 256), I32),
            pltpu.VMEM((NY, NB, 256), I32),
            pltpu.VMEM((NB, 128), I32),
            pltpu.SMEM((NB, 256), I32),
            pltpu.SMEM((NY, NB, 256), I32),
            pltpu.SMEM((NB, 128), I32),
            pltpu.VMEM((NB, 8, TOPB * BLK), F32),
            pltpu.VMEM((TOK, 128), F32),
            pltpu.VMEM((TOK, 128), F32),
            pltpu.VMEM((NB, TOK, 128), BF16),
            pltpu.VMEM((TOPB * BLK, 256), BF16),
            pltpu.VMEM((TOK, 512), BF16),
            pltpu.VMEM((TOK, 256), F32),
            pltpu.VMEM((TOK, 512), BF16),
            pltpu.VMEM((TOK, 512), BF16),
            dma((12,)),
            dma((5,)),
            dma((1,)), dma((1,)),
            dma((NY,)), dma((NY,)),
            dma((8,)), dma((8,)),
            dma((6,)), dma((6,)),
            dma((NZ * NY,)), dma((NZ * NY,)),
            dma((2,)), dma((2,)),
        ],
        compiler_params=pltpu.CompilerParams(
            collective_id=0, has_side_effects=True, vmem_limit_bytes=48 * 1024 * 1024
        ),
        name="fused",
    )(
        tokens.reshape(TOK, 512),
        norm_gain.reshape(1, 1024),
        w_query,
        w_key,
        w_value,
        q_gain.reshape(1, HD),
        k_gain.reshape(1, HD),
        w_out,
        chosen.reshape(NB, TOPB),
    )
    return mixed.reshape(1, TOK, 512), logs.reshape(1, HEADS, TOK)


def solution(mesh):
    return jax.shard_map(
        body,
        mesh=mesh,
        in_specs=(
            P("dp", "kv", "tp"), P(), P(None, "tp"), P(None, "tp"), P(None, "tp"),
            P(), P(), P("tp", None), P("dp", "kv", None),
        ),
        out_specs=(P("dp", "kv", "tp"), P("dp", "tp", "kv")),
        check_vma=False,
    )
```

time: 284 us -> 54.6 us (0.19)
  matrix products: 105 us -> 0 us
  waiting for transfers between devices: 82.6 us -> 0 us
  Pallas kernels: 0 us -> 46.4 us
  other arithmetic: 42.3 us -> 0 us
  blocking collectives: 25.5 us -> 0 us
  between operations: 14 us -> 0.68 us
  loops' own time: 2.92 us -> 0 us
    dot_general x68 -> x0, matrix products: 105 us -> none  [the longest x32 55.8 us: absorb(): jnp.einsum('sbqkgd,snkd->skgbqn', queries, span_keys, preferred_element_t...]
    all_gather x2 -> x0, waiting for transfers between devices: 66.4 us -> none  [whole_of(): result = lax.all_gather(result, axes[number], axis=dim, tiled=True)]
    pallas_call x0 -> x1, Pallas kernels: none -> 46.4 us  [body(): pl.pallas_call(kernel, out_shape=(jax.ShapeDtypeStruct((TOK, 512), BF16),...]
    another operation x32 -> x0, other arithmetic: 26.6 us -> none
    all_gather x3 -> x0, blocking collectives: 25.5 us -> none  [the longest x2 20.2 us: whole_of(): result = lax.all_gather(result, axes[number], axis=dim, tiled=True)]
    reduce_scatter x1 -> x0, waiting for transfers between devices: 16.2 us -> none  [body(): lax.psum_scatter(project().astype(jnp.bfloat16), 'tp', scatter_dimension=...]
    unnamed x14 -> x20, local copies, waits for them, and re-layouts: 0.15 us -> 7.28 us
    convert_element_type x35 -> x0, other arithmetic: 4.77 us -> none  [the longest x32 3.22 us: absorb(): offset.astype(jnp.float32)[:, None, None]]
  transfers between devices with their start and end apart: 3 -> 0, of which waited for: 3 -> 0; matrix products, arithmetic and copies ran while one was open for 2% -> 0% of each run, Pallas kernels for 0% -> 0%
where the time goes in v1:
time: 54.6 us; the launch traced here: 54.3 us
  Pallas kernels  46.4 us (85%)
  local copies, waits for them, and re-layouts  7.28 us (13%)
  between operations  0.68 us (1%)
    pallas_call x1, Pallas kernels, body(): pl.pallas_call(kernel, out_shape=(jax.ShapeDtypeStruct((TOK, 512), BF16),...  46.4 us
    unnamed x20, local copies, waits for them, and re-layouts  7.28 us

profile of v1, /device:TPU:1, one launch (start us, length us, event | category | flops | bytes accessed | tf_op | source)
XLA Modules:
  0.0 54.3 jit_solution(2642647146183836411)
XLA Ops:
  0.6 0.0 copy-start.6
  0.6 0.0 copy-start.5
  0.7 0.0 copy-start.7
  0.7 0.0 copy-start.8
  0.7 0.6 %copy-done.6 = s32[1,8,16]{2,1,0:T(8,128)S(1)} copy-done((s32[1,8,16]{2,1,0:T(8,128)S(1)}, s32[1,8,16]{2,1,0:T(8,128)}, u32[]{:S(2)}) %copy-start.6) | copy-done | bytes 536
  1.3 0.0 copy-done.5
  1.3 0.0 copy-done.7
  1.3 0.0 copy-done.8
  1.3 0.0 copy-start
  1.3 1.2 %copy-done = bf16[1024,512]{1,0:T(8,128)(2,1)S(1)} copy-done((bf16[1024,512]{1,0:T(8,128)(2,1)S(1)}, bf16[1024,512]{1,0:T(8,128)(2,1)}, u32[]{:S(2)}) %copy-start) | copy-done | bytes 1048600
  2.6 0.0 copy-start.1
  2.6 1.2 %copy-done.1 = bf16[512,1024]{1,0:T(8,128)(2,1)S(1)} copy-done((bf16[512,1024]{1,0:T(8,128)(2,1)S(1)}, bf16[512,1024]{1,0:T(8,128)(2,1)}, u32[]{:S(2)}) %copy-start.1) | copy-done | bytes 1048600
  3.8 0.0 copy-start.2
  3.8 0.9 %copy-done.2 = bf16[1,256,512]{2,1,0:T(8,128)(2,1)S(1)} copy-done((bf16[1,256,512]{2,1,0:T(8,128)(2,1)S(1)}, bf16[1,256,512]{2,1,0:T(8,128)(2,1)}, u32[]{:S(2)}) %copy-start.2) | copy-done | bytes 262168
  4.7 0.0 copy-start.3
  4.7 0.9 %copy-done.3 = bf16[1024,128]{1,0:T(8,128)(2,1)S(1)} copy-done((bf16[1024,128]{1,0:T(8,128)(2,1)S(1)}, bf16[1024,128]{1,0:T(8,128)(2,1)}, u32[]{:S(2)}) %copy-start.3) | copy-done | bytes 262168
  5.7 0.0 copy-start.4
  5.7 0.9 %copy-done.4 = bf16[1024,128]{1,0:T(8,128)(2,1)S(1)} copy-done((bf16[1024,128]{1,0:T(8,128)(2,1)S(1)}, bf16[1024,128]{1,0:T(8,128)(2,1)}, u32[]{:S(2)}) %copy-start.4) | copy-done | bytes 262168
  6.6 46.4 %fused.1 = (bf16[256,512]{1,0:T(8,128)(2,1)S(1)}, f32[8,256]{1,0:T(8,128)S(1)}) custom-call(bf16[256,512]{1,0:T(8,128)(2,1)S(1)} %bitcast.8, f32[1,1024]{1,0:T(1,128)S(1)} %bitcast.10, bf16[1024,512]{1,0:T(8,128)(2,1)S(1)} %copy-done, bf16[1024,128]{1,0:T(8,128)(2,1)S(1)} %copy-done.3, bf16[1024,128]{1,0:T(8,128)(2,1)S(1)} %copy-done.4, ...), custom_call_target="tpu_custom_call" | custom-call | tf_op jit(solution)/shard_map/fused/pallas_call | solution.py:365
  53.0 0.7 %copy.13 = bf16[1,256,512]{2,1,0:T(8,128)(2,1)} copy(bf16[1,256,512]{2,1,0:T(8,128)(2,1)S(1)} %bitcast.7) | data formatting | bytes 524288
  53.8 0.6 %copy.14 = f32[1,8,256]{2,1,0:T(8,128)} copy(f32[1,8,256]{2,1,0:T(8,128)S(1)} %bitcast.9) | data formatting | bytes 16384
Async XLA Ops:
  0.6 0.7 %copy-start.6 = (s32[1,8,16]{2,1,0:T(8,128)S(1)}, s32[1,8,16]{2,1,0:T(8,128)}, u32[]{:S(2)}) copy-start(s32[1,8,16]{2,1,0:T(8,128)} %param.17) | copy-start | bytes 1540
  0.6 0.7 %copy-start.5 = (f32[1024]{0:T(1024)S(1)}, f32[1024]{0:T(1024)}, u32[]{:S(2)}) copy-start(f32[1024]{0:T(1024)} %param.10) | copy-start | bytes 12292
  0.7 0.7 %copy-start.7 = (f32[64]{0:T(128)S(1)}, f32[64]{0:T(128)}, u32[]{:S(2)}) copy-start(f32[64]{0:T(128)} %param.14) | copy-start | bytes 772
  0.7 0.7 %copy-start.8 = (f32[64]{0:T(128)S(1)}, f32[64]{0:T(128)}, u32[]{:S(2)}) copy-start(f32[64]{0:T(128)} %param.15) | copy-start | bytes 772
  1.3 1.2 %copy-start = (bf16[1024,512]{1,0:T(8,128)(2,1)S(1)}, bf16[1024,512]{1,0:T(8,128)(2,1)}, u32[]{:S(2)}) copy-start(bf16[1024,512]{1,0:T(8,128)(2,1)} %wq.1) | copy-start | bytes 3145732
  2.6 1.2 %copy-start.1 = (bf16[512,1024]{1,0:T(8,128)(2,1)S(1)}, bf16[512,1024]{1,0:T(8,128)(2,1)}, u32[]{:S(2)}) copy-start(bf16[512,1024]{1,0:T(8,128)(2,1)} %wo.1) | copy-start | bytes 3145732
  3.8 0.9 %copy-start.2 = (bf16[1,256,512]{2,1,0:T(8,128)(2,1)S(1)}, bf16[1,256,512]{2,1,0:T(8,128)(2,1)}, u32[]{:S(2)}) copy-start(bf16[1,256,512]{2,1,0:T(8,128)(2,1)} %param.9) | copy-start | bytes 786436
  4.7 0.9 %copy-start.3 = (bf16[1024,128]{1,0:T(8,128)(2,1)S(1)}, bf16[1024,128]{1,0:T(8,128)(2,1)}, u32[]{:S(2)}) copy-start(bf16[1024,128]{1,0:T(8,128)(2,1)} %wk.1) | copy-start | bytes 786436
  5.7 0.9 %copy-start.4 = (bf16[1024,128]{1,0:T(8,128)(2,1)S(1)}, bf16[1024,128]{1,0:T(8,128)(2,1)}, u32[]{:S(2)}) copy-start(bf16[1024,128]{1,0:T(8,128)(2,1)} %wv.1) | copy-start | bytes 786436
